TPU v7x, 32 devices: a whole 2x2x4 slice. The times are simulated.
32 devices in a mesh: sp: 4 (over y, core), dp: 8 (over z, x).
Axes of the slice: x: 2, y: 2, z: 4, core: 2. Of those that a mesh axis runs over, the one named last changes fastest.
Arguments:
- queries: bfloat16 [8, 1024, 1024], P('dp', 'sp'), may hold values from -250 to 250
- keys: bfloat16 [8, 1024, 1024], P('dp', 'sp'), may hold values from -6 to 6
- values: bfloat16 [8, 1024, 1024], P('dp', 'sp'), may hold values from -6 to 6
- cum_gate: float32 [8, 16, 1024], P('dp', 'sp'), may hold values from -1024 to 0, as said below
- out_weight: bfloat16 [1024, 2112], P(None, 'dp'), may hold values from -1.5 to 1.5
Outputs:
- mixed: bfloat16 [8, 1024, 2112], P('dp', 'sp')
Inputs may be any that keep to these rules, and one draw needn't show every extreme that they name: `cum_gate`: within each head the entries do not rise along positions.
All inputs are finite; a program needn't handle non-finite values.
Results may differ from a plain program's by a relative error of at most 0.0053.
Values may be sent and summed in bfloat16 or wider, within the bound.
A program may use at most 64 MiB of HBM per device.

v0:
```python
import functools
import math

import jax
import jax.numpy as jnp
from jax import lax
from jax.experimental import pallas as pl
from jax.experimental.pallas import tpu as pltpu
from jax.sharding import PartitionSpec as P

LANES = 128
SUBLANES = 16
MESH = pl.DeviceIdType.MESH


def ring_index(position, n):
    upper = position // (n // 2)
    return (1 - upper) * (2 * position) + upper * (2 * (n - 1 - position) + 1)


def fused_kernel(
    sp, dp, depth, q, k, v, gate, w, tail, out,
    qg, kg, vg, og, attended, wg,
    qkv_send, qkv_recv, qkv_local, out_send, out_recv, out_local,
    ring_send, ring_recv, pair_send, pair_recv, own_sem,
):
    tokens, width = q.shape
    group = width // sp
    pairs = group // LANES
    per_pair = LANES // depth
    half_rows = width // 2
    main = wg.shape[3]
    rows = wg.shape[2]
    tail_rows = rows - half_rows
    columns = w.shape[1]
    tail_columns = columns - main
    steps = dp // 2
    cut = -(-(rows // 2) // SUBLANES) * SUBLANES
    me = lax.axis_index("sp")
    mine = lax.axis_index("dp")
    core = lax.rem(me, 2)
    partner = me + 1 - 2 * core
    odd = lax.rem(mine, 2)
    position = (1 - odd) * (mine // 2) + odd * (dp - 1 - mine // 2)
    right = ring_index(lax.rem(position + 1, dp), dp)
    left = ring_index(lax.rem(position + dp - 1, dp), dp)

    barrier = pltpu.get_barrier_semaphore()
    for d in range(1, sp):
        pl.semaphore_signal(
            barrier, inc=1, device_id=(lax.rem(me + d, sp), mine), device_id_type=MESH
        )
    for side in (left, right):
        pl.semaphore_signal(barrier, inc=1, device_id=(me, side), device_id_type=MESH)

    own_copies = []
    for half in range(2):
        own_copies.append(pltpu.make_async_copy(
            w.at[pl.ds(half * half_rows, half_rows), pl.ds(0, main)],
            wg.at[mine, half, pl.ds(0, half_rows)], own_sem.at[half]))
        own_copies.append(pltpu.make_async_copy(
            tail.at[half], wg.at[mine, half, pl.ds(half_rows, tail_rows)],
            own_sem.at[2 + half]))
    local_copies = {}
    arrays = ((q, qg), (k, kg), (v, vg))
    for p in range(pairs):
        for a, (source, target) in enumerate(arrays):
            local_copies[p, a] = pltpu.make_async_copy(
                source.at[:, pl.ds(pl.multiple_of(me * group + p * LANES, LANES), LANES)],
                target.at[p, pl.ds(pl.multiple_of(me * tokens, tokens), tokens), :],
                qkv_local.at[p, a])
    pl.semaphore_wait(barrier, sp + 1)

    qkv_copies = {}
    order = [2, 1, 3] if sp == 4 else list(range(1, sp))

    def send_pair(p):
        for a, (source, target) in enumerate(arrays):
            for d in order:
                peer = lax.rem(me + d, sp)
                copy = pltpu.make_async_remote_copy(
                    src_ref=source.at[:, pl.ds(pl.multiple_of(peer * group + p * LANES, LANES), LANES)],
                    dst_ref=target.at[p, pl.ds(pl.multiple_of(me * tokens, tokens), tokens), :],
                    send_sem=qkv_send.at[p, a, d - 1],
                    recv_sem=qkv_recv.at[p, a, d - 1],
                    device_id=(peer, mine),
                    device_id_type=MESH,
                )
                copy.start()
                qkv_copies[p, a, d] = copy

    ring_copies = {}
    pair_copies = {}

    def ring_slice(owner, side, step):
        if step < steps - 1:
            return wg.at[owner, core]
        if side == 0:
            return wg.at[owner, core, pl.ds(0, cut)]
        return wg.at[owner, core, pl.ds(cut, rows - cut)]

    def start_ring(key, source, target, side, slot):
        copy = pltpu.make_async_remote_copy(
            src_ref=source, dst_ref=target,
            send_sem=ring_send.at[side, slot], recv_sem=ring_recv.at[side, slot],
            device_id=(me, right if side == 0 else left), device_id_type=MESH)
        copy.start()
        ring_copies[key] = copy

    def ring_first():
        for side in range(2):
            start_ring((side, 0), w.at[pl.ds(pl.multiple_of(core * half_rows, half_rows), half_rows), pl.ds(0, main)],
                       wg.at[mine, core, pl.ds(0, half_rows)], side, 0)
            start_ring((side, steps), tail.at[core],
                       wg.at[mine, core, pl.ds(half_rows, tail_rows)], side, steps)

    def ring_step(step):
        for side in range(2):
            ring_copies[side, step].wait_recv()
            if step == 0:
                ring_copies[side, steps].wait_recv()
            shift = dp - 1 - step if side == 0 else 1 + step
            owner = ring_index(lax.rem(position + shift, dp), dp)
            if step + 1 < steps:
                piece = ring_slice(owner, side, step + 1)
                start_ring((side, step + 1), piece, piece, side, step + 1)
            piece = ring_slice(owner, side, step)
            copy = pltpu.make_async_remote_copy(
                src_ref=piece, dst_ref=piece,
                send_sem=pair_send.at[side, step], recv_sem=pair_recv.at[side, step],
                device_id=(partner, mine), device_id_type=MESH)
            copy.start()
            pair_copies[side, step] = copy

    send_pair(0)
    ring_first()
    for p in range(1, pairs):
        send_pair(p)
    for copy in local_copies.values():
        copy.start()
    for copy in own_copies:
        copy.start()

    log2e = math.log2(math.e)
    factor = depth ** -0.5 * log2e
    gates = gate[...] * log2e
    gates_t = jnp.transpose(gates)
    lane = lax.broadcasted_iota(jnp.int32, (tokens, LANES), 1) // depth
    diagonal = (
        lax.broadcasted_iota(jnp.int32, (tokens, tokens), 1)
        <= lax.broadcasted_iota(jnp.int32, (tokens, tokens), 0)
    )

    def attend_block(p, i):
        keys = (i + 1) * tokens
        query = qg[p, i * tokens:keys, :]
        key = kg[p, 0:keys, :]
        value = vg[p, 0:keys, :]
        result = jnp.zeros((tokens, LANES), jnp.float32)
        for j in range(per_pair):
            h = p * per_pair + j
            masked = jnp.where(lane == j, query, jnp.zeros_like(query))
            logits = lax.dot_general(
                masked, key, (((1,), (1,)), ((), ())), preferred_element_type=jnp.float32
            ) * factor
            logits = logits + (gates_t[i * tokens:keys, h:h + 1] - gates[h:h + 1, 0:keys])
            last = jnp.where(diagonal, logits[:, i * tokens:], -jnp.inf)
            logits = jnp.concatenate([logits[:, :i * tokens], last], axis=1) if i else last
            top = jnp.max(logits, axis=1, keepdims=True)
            scores = jnp.exp2(logits - top)
            total = jnp.sum(scores, axis=1, keepdims=True)
            weighted = jnp.dot(scores.astype(jnp.bfloat16), value, preferred_element_type=jnp.float32)
            result = jnp.where(lane == j, weighted / total, result)
        og[p, i * tokens:keys, :] = result.astype(jnp.bfloat16)

    out_copies = []

    def send_out(p):
        for d in order:
            peer = lax.rem(me + d, sp)
            copy = pltpu.make_async_remote_copy(
                src_ref=og.at[p, pl.ds(pl.multiple_of(peer * tokens, tokens), tokens), :],
                dst_ref=attended.at[:, pl.ds(pl.multiple_of(me * group + p * LANES, LANES), LANES)],
                send_sem=out_send.at[p, d - 1], recv_sem=out_recv.at[p, d - 1],
                device_id=(peer, mine), device_id_type=MESH)
            copy.start()
            out_copies.append(copy)
        copy = pltpu.make_async_copy(
            og.at[p, pl.ds(pl.multiple_of(me * tokens, tokens), tokens), :],
            attended.at[:, pl.ds(pl.multiple_of(me * group + p * LANES, LANES), LANES)],
            out_local.at[p])
        copy.start()
        own_copies.append(copy)

    done = 0
    for p in range(pairs):
        if done < steps:
            ring_step(done)
            done += 1
        for a in range(3):
            local_copies[p, a].wait()
            for d in order:
                qkv_copies[p, a, d].wait_recv()
        for i in range(sp):
            if i == sp // 2 and p == pairs - 1 and done < steps:
                ring_step(done)
                done += 1
            attend_block(p, i)
        send_out(p)
    while done < steps:
        ring_step(done)
        done += 1

    for copy in own_copies:
        copy.wait()
    for copy in out_copies:
        copy.wait()
    for copy in pair_copies.values():
        copy.wait()

    tail_first = jnp.zeros((tokens, dp * tail_rows), jnp.float32)
    tail_second = jnp.zeros((tokens, dp * tail_rows), jnp.float32)
    quarter = half_rows // 2
    nt = (((1,), (1,)), ((), ()))
    for half in range(2):
        packed = wg[:, half, half_rows:, :].reshape(dp * tail_rows, main)
        tail_first += lax.dot_general(
            attended[:, half * half_rows:half * half_rows + quarter], packed, nt,
            preferred_element_type=jnp.float32)
        tail_second += lax.dot_general(
            attended[:, half * half_rows + quarter:(half + 1) * half_rows], packed, nt,
            preferred_element_type=jnp.float32)
    for owner in range(dp):
        product = jnp.dot(
            attended[:, :half_rows], wg[owner, 0, :half_rows, :], preferred_element_type=jnp.float32)
        product += jnp.dot(
            attended[:, half_rows:], wg[owner, 1, :half_rows, :], preferred_element_type=jnp.float32)
        first = owner * tail_rows
        second = first + tail_columns
        end = (
            tail_first[:, first:first + tail_columns]
            + tail_second[:, second:second + tail_columns]
        )
        whole = jnp.concatenate([product, end], axis=1).astype(jnp.bfloat16)
        out[:, owner * columns:(owner + 1) * columns] = whole

    for copy in qkv_copies.values():
        copy.wait_send()
    for copy in ring_copies.values():
        copy.wait_send()


def fused(sp, dp, depth, q, k, v, gate, w):
    tokens, width = q.shape
    length = tokens * sp
    columns = w.shape[1]
    main = columns // LANES * LANES
    half = width // 2
    tail = w[:, main:].reshape(2, 2, half // 2, columns - main)
    tail = tail.transpose(0, 1, 3, 2).reshape(2, 2 * (columns - main), main)
    group = width // sp
    pairs = group // LANES
    steps = dp // 2
    any_spec = pl.BlockSpec(memory_space=pl.ANY)
    vmem_spec = pl.BlockSpec(memory_space=pltpu.VMEM)
    dma = pltpu.SemaphoreType.DMA
    gathered = pltpu.VMEM((pairs, length, LANES), jnp.bfloat16)
    return pl.pallas_call(
        functools.partial(fused_kernel, sp, dp, depth),
        out_shape=jax.ShapeDtypeStruct((tokens, columns * dp), jnp.bfloat16),
        in_specs=[any_spec, any_spec, any_spec, vmem_spec, any_spec, vmem_spec],
        out_specs=vmem_spec,
        scratch_shapes=[
            gathered, gathered, gathered, gathered,
            pltpu.VMEM((tokens, width), jnp.bfloat16),
            pltpu.VMEM((dp, 2, half + tail.shape[1], main), jnp.bfloat16),
            dma((pairs, 3, sp - 1)), dma((pairs, 3, sp - 1)), dma((pairs, 3)),
            dma((pairs, sp - 1)), dma((pairs, sp - 1)), dma((pairs,)),
            dma((2, steps + 1)), dma((2, steps + 1)),
            dma((2, steps)), dma((2, steps)), dma((4,)),
        ],
        compiler_params=pltpu.CompilerParams(
            collective_id=0, has_side_effects=True, vmem_limit_bytes=48 * 1024 * 1024),
    )(q, k, v, gate, w, tail)


def fits(sp, dp, tokens, width, depth, columns):
    main = columns // LANES * LANES
    return (
        sp % 2 == 0 and dp % 2 == 0 and dp >= 4
        and (width // sp) % LANES == 0 and LANES % depth == 0
        and tokens * sp <= 1024 and tokens % LANES == 0
        and main * 4 == width and columns > main
        and 2 * (columns - main) == SUBLANES
    )


def attend(query_all, key_all, value_all, gate_all):
    length, width = query_all.shape
    heads = gate_all.shape[0]
    depth = width // heads
    block_rows = min(512, length)
    block_count = length // block_rows
    score_scale = depth ** (-0.5)
    query_blocks = query_all.reshape(block_count, block_rows, heads, depth)
    key_blocks = key_all.reshape(block_count, block_rows, heads, depth)
    value_blocks = value_all.reshape(block_count, block_rows, heads, depth)
    gate_blocks = gate_all.reshape(heads, block_count, block_rows).transpose(1, 0, 2)
    offsets = jnp.arange(block_rows, dtype=jnp.int32)

    def one_block(block_index):
        query_part = lax.dynamic_index_in_dim(query_blocks, block_index, 0, keepdims=False)
        gate_part = lax.dynamic_index_in_dim(gate_blocks, block_index, 0, keepdims=False)
        query_rows = block_index * block_rows + offsets

        def key_step(key_block, carry):
            running_max, running_sum, weighted = carry
            key_part = lax.dynamic_index_in_dim(key_blocks, key_block, 0, keepdims=False)
            value_part = lax.dynamic_index_in_dim(value_blocks, key_block, 0, keepdims=False)
            gate_keys = lax.dynamic_index_in_dim(gate_blocks, key_block, 0, keepdims=False)
            logits = (
                jnp.einsum("qhe,khe->hqk", query_part, key_part, preferred_element_type=jnp.float32)
                * score_scale
            )
            logits = logits + gate_part[:, :, None] - gate_keys[:, None, :]
            key_rows = key_block * block_rows + offsets
            allowed = key_rows[None, :] <= query_rows[:, None]
            logits = jnp.where(allowed[None], logits, -jnp.inf)
            new_max = jnp.maximum(running_max, jnp.max(logits, axis=-1))
            scores = jnp.exp(logits - new_max[..., None])
            factor = jnp.exp(running_max - new_max)
            running_sum = running_sum * factor + jnp.sum(scores, axis=-1)
            weighted = weighted * factor[..., None] + jnp.einsum(
                "hqk,khe->hqe",
                scores.astype(jnp.bfloat16),
                value_part,
                preferred_element_type=jnp.float32,
            )
            return (new_max, running_sum, weighted)

        start_state = (
            jnp.full((heads, block_rows), -jnp.inf, jnp.float32),
            jnp.zeros((heads, block_rows), jnp.float32),
            jnp.zeros((heads, block_rows, depth), jnp.float32),
        )
        final_max, final_sum, weighted = lax.fori_loop(0, block_index + 1, key_step, start_state)
        result = weighted / final_sum[..., None]
        return result.transpose(1, 0, 2).astype(jnp.bfloat16)

    outputs = lax.map(one_block, jnp.arange(block_count, dtype=jnp.int32))
    return outputs.reshape(length, width)


def body(queries, keys, values, cum_gate, out_weight):
    sp, dp = lax.axis_size("sp"), lax.axis_size("dp")
    tokens, width = queries.shape[1:]
    depth = width // (cum_gate.shape[1] * sp)
    if fits(sp, dp, tokens, width, depth, out_weight.shape[1]):
        mixed = fused(sp, dp, depth, queries[0], keys[0], values[0], cum_gate[0], out_weight)
        return mixed[None]
    query_heads, key_heads, value_heads = (
        lax.all_to_all(queries, "sp", split_axis=2, concat_axis=1, tiled=True),
        lax.all_to_all(keys, "sp", split_axis=2, concat_axis=1, tiled=True),
        lax.all_to_all(values, "sp", split_axis=2, concat_axis=1, tiled=True),
    )
    local_out = attend(query_heads[0], key_heads[0], value_heads[0], cum_gate[0])
    attended = lax.all_to_all(local_out[None], "sp", split_axis=1, concat_axis=2, tiled=True)[0]
    group_rows = attended.shape[1] // lax.axis_size("sp")
    own_rows = lax.dynamic_slice_in_dim(
        out_weight, lax.axis_index("sp") * group_rows, group_rows, 0
    )
    full_rows = lax.all_gather(own_rows, "dp", axis=1, tiled=True)
    whole_weight = lax.all_gather(full_rows, "sp", axis=0, tiled=True)
    mixed = jnp.dot(attended, whole_weight, preferred_element_type=jnp.float32)
    return mixed.astype(jnp.bfloat16)[None]


def solution(mesh):
    in_specs = (
        P("dp", "sp", None),
        P("dp", "sp", None),
        P("dp", "sp", None),
        P("dp", "sp", None),
        P(None, "dp"),
    )
    out_specs = P("dp", "sp", None)
    return jax.shard_map(body, mesh=mesh, in_specs=in_specs, out_specs=out_specs, check_vma=False)
```

profile of v0, /device:TPU:0, one launch (start us, length us, event | category | flops | bytes accessed | tf_op | source)
XLA Modules:
  0.0 39.2 jit_solution(3896398497616375754)
XLA Ops:
  0.0 0.0 copy-start.3
  0.0 0.0 copy-start.1
  0.0 0.0 copy-start
  0.0 0.8 %slice.3 = bf16[1024,8]{0,1:T(8,128)(2,1)S(1)} slice(bf16[1024,264]{0,1:T(8,128)(2,1)} %param.9), slice={[0:1024], [256:264]} | slice | bytes 32768 | tf_op jit(solution)/shard_map/slice | solution.py:259
  0.8 1.4 %copy.6.w = bf16[1024,264]{1,0:T(8,128)(2,1)S(1)} copy(bf16[1024,264]{0,1:T(8,128)(2,1)} %param.9) | data formatting | bytes 1081344 | tf_op args[4]
  2.2 0.0 copy-done.3
  2.2 0.0 copy-done.1
  2.2 0.0 copy-done
  2.3 0.0 copy-start.2
  2.3 1.0 %copy-done.2 = bf16[1,256,1024]{2,1,0:T(8,128)(2,1)S(1)} copy-done((bf16[1,256,1024]{2,1,0:T(8,128)(2,1)S(1)}, bf16[1,256,1024]{2,1,0:T(8,128)(2,1)}, u32[]{:S(2)}) %copy-start.2) | copy-done | bytes 524312
  3.3 34.6 %shard_map.55 = bf16[256,2112]{1,0:T(8,128)(2,1)S(1)} custom-call(bf16[256,1024]{1,0:T(8,128)(2,1)S(1)} %bitcast.11, bf16[256,1024]{1,0:T(8,128)(2,1)S(1)} %bitcast.12, bf16[256,1024]{1,0:T(8,128)(2,1)S(1)} %bitcast.13, f32[4,1024]{1,0:T(4,128)S(1)} %bitcast.15, bf16[1024,264]{1,0:T(8,128)(2,1)S(1)} %copy.6.w, bf16[2,16,256]{2,1,0:T(8,128)(2,1)S(1)} %bitcast.14), custom_call_target="tpu_custom_call" | custom-call | tf_op jit(solution)/shard_map/pallas_call | solution.py:268
  37.9 1.4 %copy.7 = bf16[1,256,2112]{1,2,0:T(8,128)(2,1)} copy(bf16[1,256,2112]{2,1,0:T(8,128)(2,1)S(1)} %bitcast.10) | data formatting | bytes 2162688 | tf_op jit(solution)/shard_map/broadcast_in_dim | solution.py:360
Async XLA Ops:
  0.0 2.2 %copy-start.3 = (f32[1,4,1024]{2,1,0:T(4,128)S(1)}, f32[1,4,1024]{2,1,0:T(4,128)}, u32[]{:S(2)}) copy-start(f32[1,4,1024]{2,1,0:T(4,128)} %param.8) | copy-start | bytes 49156
  0.0 2.2 %copy-start.1 = (bf16[1,256,1024]{2,1,0:T(8,128)(2,1)S(1)}, bf16[1,256,1024]{2,1,0:T(8,128)(2,1)}, u32[]{:S(2)}) copy-start(bf16[1,256,1024]{2,1,0:T(8,128)(2,1)} %param.6) | copy-start | bytes 1572868
  0.0 2.2 %copy-start = (bf16[1,256,1024]{2,1,0:T(8,128)(2,1)S(1)}, bf16[1,256,1024]{2,1,0:T(8,128)(2,1)}, u32[]{:S(2)}) copy-start(bf16[1,256,1024]{2,1,0:T(8,128)(2,1)} %param.5) | copy-start | bytes 1572868
  2.3 1.0 %copy-start.2 = (bf16[1,256,1024]{2,1,0:T(8,128)(2,1)S(1)}, bf16[1,256,1024]{2,1,0:T(8,128)(2,1)}, u32[]{:S(2)}) copy-start(bf16[1,256,1024]{2,1,0:T(8,128)(2,1)} %param.7) | copy-start | bytes 1572868
where the time goes:
time: 39.5 us; the launch traced here: 39.2 us
  Pallas kernels  34.6 us (88%)
  local copies, waits for them, and re-layouts  4.61 us (12%)
    pallas_call x1, Pallas kernels, fused(): pl.pallas_call(functools.partial(fused_kernel, sp, dp, depth), out_shape=...  34.6 us
    unnamed x9, local copies, waits for them, and re-layouts  2.45 us
    broadcast_in_dim x1, local copies, waits for them, and re-layouts, body(): return mixed[None]  1.35 us
    slice x1, local copies, waits for them, and re-layouts, fused(): tail = w[:, main:].reshape(2, 2, half // 2, columns - main)  0.81 us

commit v1 on v0

--- a/solution.py
+++ b/solution.py
@@ -19,7 +19,7 @@
 
 
 def fused_kernel(
-    sp, dp, depth, q, k, v, gate, w, tail, out,
+    sp, dp, depth, q, k, v, gate, w, out,
     qg, kg, vg, og, attended, wg,
     qkv_send, qkv_recv, qkv_local, out_send, out_recv, out_local,
     ring_send, ring_recv, pair_send, pair_recv, own_sem,
@@ -28,14 +28,10 @@
     group = width // sp
     pairs = group // LANES
     per_pair = LANES // depth
-    half_rows = width // 2
-    main = wg.shape[3]
-    rows = wg.shape[2]
-    tail_rows = rows - half_rows
-    columns = w.shape[1]
-    tail_columns = columns - main
+    half = width // 2
+    columns = w.shape[0]
     steps = dp // 2
-    cut = -(-(rows // 2) // SUBLANES) * SUBLANES
+    cut = -(-(columns // 2) // SUBLANES) * SUBLANES
     me = lax.axis_index("sp")
     mine = lax.axis_index("dp")
     core = lax.rem(me, 2)
@@ -53,14 +49,7 @@
     for side in (left, right):
         pl.semaphore_signal(barrier, inc=1, device_id=(me, side), device_id_type=MESH)
 
-    own_copies = []
-    for half in range(2):
-        own_copies.append(pltpu.make_async_copy(
-            w.at[pl.ds(half * half_rows, half_rows), pl.ds(0, main)],
-            wg.at[mine, half, pl.ds(0, half_rows)], own_sem.at[half]))
-        own_copies.append(pltpu.make_async_copy(
-            tail.at[half], wg.at[mine, half, pl.ds(half_rows, tail_rows)],
-            own_sem.at[2 + half]))
+    own_copies = [pltpu.make_async_copy(w, wg.at[mine], own_sem.at[0])]
     local_copies = {}
     arrays = ((q, qg), (k, kg), (v, vg))
     for p in range(pairs):
@@ -92,12 +81,14 @@
     ring_copies = {}
     pair_copies = {}
 
+    lanes = pl.ds(pl.multiple_of(core * half, half), half)
+
     def ring_slice(owner, side, step):
         if step < steps - 1:
-            return wg.at[owner, core]
+            return wg.at[owner, :, lanes]
         if side == 0:
-            return wg.at[owner, core, pl.ds(0, cut)]
-        return wg.at[owner, core, pl.ds(cut, rows - cut)]
+            return wg.at[owner, pl.ds(0, cut), lanes]
+        return wg.at[owner, pl.ds(cut, columns - cut), lanes]
 
     def start_ring(key, source, target, side, slot):
         copy = pltpu.make_async_remote_copy(
@@ -109,16 +100,11 @@
 
     def ring_first():
         for side in range(2):
-            start_ring((side, 0), w.at[pl.ds(pl.multiple_of(core * half_rows, half_rows), half_rows), pl.ds(0, main)],
-                       wg.at[mine, core, pl.ds(0, half_rows)], side, 0)
-            start_ring((side, steps), tail.at[core],
-                       wg.at[mine, core, pl.ds(half_rows, tail_rows)], side, steps)
+            start_ring((side, 0), w.at[:, lanes], wg.at[mine, :, lanes], side, 0)
 
     def ring_step(step):
         for side in range(2):
             ring_copies[side, step].wait_recv()
-            if step == 0:
-                ring_copies[side, steps].wait_recv()
             shift = dp - 1 - step if side == 0 else 1 + step
             owner = ring_index(lax.rem(position + shift, dp), dp)
             if step + 1 < steps:
@@ -218,31 +204,11 @@
     for copy in pair_copies.values():
         copy.wait()
 
-    tail_first = jnp.zeros((tokens, dp * tail_rows), jnp.float32)
-    tail_second = jnp.zeros((tokens, dp * tail_rows), jnp.float32)
-    quarter = half_rows // 2
     nt = (((1,), (1,)), ((), ()))
-    for half in range(2):
-        packed = wg[:, half, half_rows:, :].reshape(dp * tail_rows, main)
-        tail_first += lax.dot_general(
-            attended[:, half * half_rows:half * half_rows + quarter], packed, nt,
-            preferred_element_type=jnp.float32)
-        tail_second += lax.dot_general(
-            attended[:, half * half_rows + quarter:(half + 1) * half_rows], packed, nt,
-            preferred_element_type=jnp.float32)
     for owner in range(dp):
-        product = jnp.dot(
-            attended[:, :half_rows], wg[owner, 0, :half_rows, :], preferred_element_type=jnp.float32)
-        product += jnp.dot(
-            attended[:, half_rows:], wg[owner, 1, :half_rows, :], preferred_element_type=jnp.float32)
-        first = owner * tail_rows
-        second = first + tail_columns
-        end = (
-            tail_first[:, first:first + tail_columns]
-            + tail_second[:, second:second + tail_columns]
-        )
-        whole = jnp.concatenate([product, end], axis=1).astype(jnp.bfloat16)
-        out[:, owner * columns:(owner + 1) * columns] = whole
+        product = lax.dot_general(
+            wg[owner], attended[...], nt, preferred_element_type=jnp.float32)
+        out[owner * columns:(owner + 1) * columns, :] = product.astype(jnp.bfloat16)
 
     for copy in qkv_copies.values():
         copy.wait_send()
@@ -253,45 +219,39 @@
 def fused(sp, dp, depth, q, k, v, gate, w):
     tokens, width = q.shape
     length = tokens * sp
-    columns = w.shape[1]
-    main = columns // LANES * LANES
-    half = width // 2
-    tail = w[:, main:].reshape(2, 2, half // 2, columns - main)
-    tail = tail.transpose(0, 1, 3, 2).reshape(2, 2 * (columns - main), main)
+    columns = w.shape[0]
     group = width // sp
     pairs = group // LANES
     steps = dp // 2
-    any_spec = pl.BlockSpec(memory_space=pl.ANY)
+    any_spec = pl.BlockSpec(memory_space=pltpu.HBM)
     vmem_spec = pl.BlockSpec(memory_space=pltpu.VMEM)
     dma = pltpu.SemaphoreType.DMA
     gathered = pltpu.VMEM((pairs, length, LANES), jnp.bfloat16)
     return pl.pallas_call(
         functools.partial(fused_kernel, sp, dp, depth),
-        out_shape=jax.ShapeDtypeStruct((tokens, columns * dp), jnp.bfloat16),
-        in_specs=[any_spec, any_spec, any_spec, vmem_spec, any_spec, vmem_spec],
+        out_shape=jax.ShapeDtypeStruct((columns * dp, tokens), jnp.bfloat16),
+        in_specs=[any_spec, any_spec, any_spec, vmem_spec, any_spec],
         out_specs=vmem_spec,
         scratch_shapes=[
             gathered, gathered, gathered, gathered,
             pltpu.VMEM((tokens, width), jnp.bfloat16),
-            pltpu.VMEM((dp, 2, half + tail.shape[1], main), jnp.bfloat16),
+            pltpu.VMEM((dp, columns, width), jnp.bfloat16),
             dma((pairs, 3, sp - 1)), dma((pairs, 3, sp - 1)), dma((pairs, 3)),
             dma((pairs, sp - 1)), dma((pairs, sp - 1)), dma((pairs,)),
-            dma((2, steps + 1)), dma((2, steps + 1)),
-            dma((2, steps)), dma((2, steps)), dma((4,)),
+            dma((2, steps)), dma((2, steps)),
+            dma((2, steps)), dma((2, steps)), dma((1,)),
         ],
         compiler_params=pltpu.CompilerParams(
             collective_id=0, has_side_effects=True, vmem_limit_bytes=48 * 1024 * 1024),
-    )(q, k, v, gate, w, tail)
+    )(q, k, v, gate, w)
 
 
 def fits(sp, dp, tokens, width, depth, columns):
-    main = columns // LANES * LANES
     return (
         sp % 2 == 0 and dp % 2 == 0 and dp >= 4
         and (width // sp) % LANES == 0 and LANES % depth == 0
         and tokens * sp <= 1024 and tokens % LANES == 0
-        and main * 4 == width and columns > main
-        and 2 * (columns - main) == SUBLANES
+        and width % (2 * LANES) == 0 and columns % 8 == 0
     )
 
 
@@ -356,8 +316,8 @@
     tokens, width = queries.shape[1:]
     depth = width // (cum_gate.shape[1] * sp)
     if fits(sp, dp, tokens, width, depth, out_weight.shape[1]):
-        mixed = fused(sp, dp, depth, queries[0], keys[0], values[0], cum_gate[0], out_weight)
-        return mixed[None]
+        mixed = fused(sp, dp, depth, queries[0], keys[0], values[0], cum_gate[0], out_weight.T)
+        return mixed.T[None]
     query_heads, key_heads, value_heads = (
         lax.all_to_all(queries, "sp", split_axis=2, concat_axis=1, tiled=True),
         lax.all_to_all(keys, "sp", split_axis=2, concat_axis=1, tiled=True),

time: 39.5 us -> 40.7 us (1.030)
  local copies, waits for them, and re-layouts: 4.61 us -> 5.87 us
    unnamed x9 -> x11, local copies, waits for them, and re-layouts: 2.45 us -> 5.87 us
    broadcast_in_dim x1 -> x0, local copies, waits for them, and re-layouts: 1.35 us -> none  [body(): return mixed[None]]
    slice x1 -> x0, local copies, waits for them, and re-layouts: 0.81 us -> none  [fused(): tail = w[:, main:].reshape(2, 2, half // 2, columns - main)]
where the time goes in v1:
time: 40.7 us; the launch traced here: 40.3 us
  Pallas kernels  34.4 us (85%)
  local copies, waits for them, and re-layouts  5.87 us (14%)
    pallas_call x1, Pallas kernels, fused(): pl.pallas_call(functools.partial(fused_kernel, sp, dp, depth), out_shape=...  34.4 us
    unnamed x11, local copies, waits for them, and re-layouts  5.87 us

profile of v1, /device:TPU:0, one launch (start us, length us, event | category | flops | bytes accessed | tf_op | source)
XLA Modules:
  0.0 40.3 jit_solution(10524337658125673136)
XLA Ops:
  0.0 0.0 copy-start
  0.0 1.0 %copy-done = bf16[1024,264]{0,1:T(8,128)(2,1)S(1)} copy-done((bf16[1024,264]{0,1:T(8,128)(2,1)S(1)}, bf16[1024,264]{0,1:T(8,128)(2,1)}, u32[]{:S(2)}) %copy-start) | copy-done | bytes 540696
  1.0 0.0 copy-start.1
  1.1 1.0 %copy-done.1 = bf16[1,256,1024]{2,1,0:T(8,128)(2,1)S(1)} copy-done((bf16[1,256,1024]{2,1,0:T(8,128)(2,1)S(1)}, bf16[1,256,1024]{2,1,0:T(8,128)(2,1)}, u32[]{:S(2)}) %copy-start.1) | copy-done | bytes 524312
  2.1 0.0 copy-start.2
  2.1 1.0 %copy-done.2 = bf16[1,256,1024]{2,1,0:T(8,128)(2,1)S(1)} copy-done((bf16[1,256,1024]{2,1,0:T(8,128)(2,1)S(1)}, bf16[1,256,1024]{2,1,0:T(8,128)(2,1)}, u32[]{:S(2)}) %copy-start.2) | copy-done | bytes 524312
  3.1 0.0 copy-start.3
  3.1 1.0 %copy-done.3 = bf16[1,256,1024]{2,1,0:T(8,128)(2,1)S(1)} copy-done((bf16[1,256,1024]{2,1,0:T(8,128)(2,1)S(1)}, bf16[1,256,1024]{2,1,0:T(8,128)(2,1)}, u32[]{:S(2)}) %copy-start.3) | copy-done | bytes 524312
  4.2 0.0 copy-start.4
  4.2 0.7 %copy-done.4 = f32[1,4,1024]{2,1,0:T(4,128)S(1)} copy-done((f32[1,4,1024]{2,1,0:T(4,128)S(1)}, f32[1,4,1024]{2,1,0:T(4,128)}, u32[]{:S(2)}) %copy-start.4) | copy-done | bytes 16408
  4.9 34.4 %shard_map.55 = bf16[2112,256]{1,0:T(8,128)(2,1)S(1)} custom-call(bf16[256,1024]{1,0:T(8,128)(2,1)S(1)} %bitcast.10, bf16[256,1024]{1,0:T(8,128)(2,1)S(1)} %bitcast.11, bf16[256,1024]{1,0:T(8,128)(2,1)S(1)} %bitcast.12, f32[4,1024]{1,0:T(4,128)S(1)} %bitcast.13, bf16[264,1024]{1,0:T(8,128)(2,1)S(1)} %bitcast.9), custom_call_target="tpu_custom_call" | custom-call | tf_op jit(solution)/shard_map/pallas_call | solution.py:230
  39.3 1.0 %copy.7 = bf16[1,256,2112]{1,2,0:T(8,128)(2,1)} copy(bf16[1,256,2112]{1,2,0:T(8,128)(2,1)S(1)} %bitcast.8) | data formatting | bytes 2162688
Async XLA Ops:
  0.0 1.0 %copy-start = (bf16[1024,264]{0,1:T(8,128)(2,1)S(1)}, bf16[1024,264]{0,1:T(8,128)(2,1)}, u32[]{:S(2)}) copy-start(bf16[1024,264]{0,1:T(8,128)(2,1)} %param.9) | copy-start | bytes 1622020
  1.0 1.0 %copy-start.1 = (bf16[1,256,1024]{2,1,0:T(8,128)(2,1)S(1)}, bf16[1,256,1024]{2,1,0:T(8,128)(2,1)}, u32[]{:S(2)}) copy-start(bf16[1,256,1024]{2,1,0:T(8,128)(2,1)} %param.5) | copy-start | bytes 1572868
  2.1 1.0 %copy-start.2 = (bf16[1,256,1024]{2,1,0:T(8,128)(2,1)S(1)}, bf16[1,256,1024]{2,1,0:T(8,128)(2,1)}, u32[]{:S(2)}) copy-start(bf16[1,256,1024]{2,1,0:T(8,128)(2,1)} %param.6) | copy-start | bytes 1572868
  3.1 1.0 %copy-start.3 = (bf16[1,256,1024]{2,1,0:T(8,128)(2,1)S(1)}, bf16[1,256,1024]{2,1,0:T(8,128)(2,1)}, u32[]{:S(2)}) copy-start(bf16[1,256,1024]{2,1,0:T(8,128)(2,1)} %param.7) | copy-start | bytes 1572868
  4.2 0.7 %copy-start.4 = (f32[1,4,1024]{2,1,0:T(4,128)S(1)}, f32[1,4,1024]{2,1,0:T(4,128)}, u32[]{:S(2)}) copy-start(f32[1,4,1024]{2,1,0:T(4,128)} %param.8) | copy-start | bytes 49156

commit v2 on v1

v2 whole, which is shorter than its diff:
```python
import functools
import math

import jax
import jax.numpy as jnp
from jax import lax
from jax.experimental import pallas as pl
from jax.experimental.pallas import tpu as pltpu
from jax.sharding import PartitionSpec as P

LANES = 128
PACK = 8
PARTS = 3
CHUNKS = 2
ONES = 16
MESH = pl.DeviceIdType.MESH


def ring_index(position, n):
    upper = position // (n // 2)
    return (1 - upper) * (2 * position) + upper * (2 * (n - 1 - position) + 1)


def spans(total, pieces):
    units = total // PACK
    cuts = [PACK * (units * i // pieces) for i in range(pieces + 1)]
    return [(cuts[i], cuts[i + 1] - cuts[i]) for i in range(pieces)]


def fused_kernel(
    dp, depth, q, k, v, gate, w, out,
    qbuf, kbuf, vbuf, gown, gbuf, bias, vt, qx, ox, lx, oin, lin, oloc, lloc, att, wg, obuf,
    load_sem, kv_send, kv_recv, gate_send, gate_recv, qx_send, qx_recv,
    ox_send, ox_recv, lx_send, lx_recv, ring_send, ring_recv, pair_send, pair_recv, out_sem,
):
    tokens, width = q.shape
    columns = w.shape[0]
    pairs = width // LANES
    per_pair = LANES // depth
    own_heads = gown.shape[0]
    heads = width // depth
    both = 2 * tokens
    steps = dp // 2
    rounds = pairs // 2
    me = lax.axis_index("sp")
    mine = lax.axis_index("dp")
    core = lax.rem(me, 2)
    side_y = me // 2
    partner = me + 1 - 2 * core
    odd = lax.rem(mine, 2)
    position = (1 - odd) * (mine // 2) + odd * (dp - 1 - mine // 2)
    right = ring_index(lax.rem(position + 1, dp), dp)
    left = ring_index(lax.rem(position + dp - 1, dp), dp)
    low = side_y == 0
    high = side_y == 1

    def local(source, target, slot):
        copy = pltpu.make_async_copy(source, target, load_sem.at[slot])
        copy.start()
        return copy

    own_rows = pl.ds(pl.multiple_of(core * tokens, tokens), tokens)
    loads = [
        local(gate, gown, 0),
        local(k, kbuf.at[own_rows], 1),
        local(v, vbuf.at[own_rows], 2),
        local(q, qbuf, 3),
        local(w, wg.at[mine], 4),
    ]

    barrier = pltpu.get_barrier_semaphore()
    for d in range(1, 4):
        pl.semaphore_signal(
            barrier, inc=1, device_id=(lax.rem(me + d, 4), mine), device_id_type=MESH)
    for side in (left, right):
        pl.semaphore_signal(barrier, inc=1, device_id=(me, side), device_id_type=MESH)
    for copy in loads:
        copy.wait()
    gbuf[me] = gown[:, pl.ds(pl.multiple_of(side_y * both, both), both)]
    pl.semaphore_wait(barrier, 5)

    def remote(source, target, send, recv, device):
        return pltpu.make_async_remote_copy(
            src_ref=source, dst_ref=target, send_sem=send, recv_sem=recv,
            device_id=device, device_id_type=MESH)

    gate_copies = []
    for d in range(1, 4):
        peer = lax.rem(me + d, 4)
        gate_copies.append(remote(
            gown.at[:, pl.ds(pl.multiple_of((peer // 2) * both, both), both)],
            gbuf.at[me], gate_send.at[d - 1], gate_recv.at[d - 1], (peer, mine)))
    kv_copies = [
        remote(ref.at[own_rows], ref.at[own_rows], kv_send.at[i], kv_recv.at[i], (partner, mine))
        for i, ref in enumerate((kbuf, vbuf))
    ]

    def q_copy(p):
        return remote(
            qbuf.at[:, pl.ds(p * LANES, LANES)], qx.at[p, core],
            qx_send.at[p], qx_recv.at[p, core], (p % 2, mine))

    for copy in gate_copies:
        copy.start()
    for copy in kv_copies:
        copy.start()

    @pl.when(high)
    def _():
        for p in range(pairs):
            q_copy(p).start()

    half = width // 2
    lanes = pl.ds(pl.multiple_of(core * half, half), half)
    chunks = spans(columns, CHUNKS)
    events = steps * CHUNKS - CHUNKS // 2 if CHUNKS > 1 else steps
    ring_copies = {}
    pair_copies = {}

    def piece(owner, chunk):
        start, size = chunks[chunk]
        return wg.at[owner, pl.ds(start, size), lanes]

    def owner_of(side, step):
        shift = dp - 1 - step if side == 0 else 1 + step
        return ring_index(lax.rem(position + shift, dp), dp)

    def carries(side, step, chunk):
        if step < steps - 1:
            return True
        return (chunk < CHUNKS // 2) == (side == 0)

    def start_ring(side, step, chunk, owner):
        if not carries(side, step, chunk):
            return
        slot = step * CHUNKS + chunk
        copy = remote(
            piece(owner, chunk), piece(owner, chunk),
            ring_send.at[side, slot], ring_recv.at[side, slot],
            (me, right if side == 0 else left))
        copy.start()
        ring_copies[side, step, chunk] = copy

    def ring_event(step, index):
        for side in range(2):
            chunk = index
            if step == steps - 1:
                chunk = index + (CHUNKS // 2) * side
            owner = owner_of(side, step)
            ring_copies[side, step, chunk].wait_recv()
            if step + 1 < steps:
                start_ring(side, step + 1, chunk, owner)
            slot = step * CHUNKS + chunk
            copy = remote(
                piece(owner, chunk), piece(owner, chunk),
                pair_send.at[side, slot], pair_recv.at[side, slot], (partner, mine))
            copy.start()
            pair_copies[side, step, chunk] = copy

    for chunk in range(CHUNKS):
        for side in range(2):
            start_ring(side, 0, chunk, mine)

    scale = depth ** -0.5 * math.log2(math.e)
    for copy in kv_copies:
        copy.wait_recv()

    def transpose_values(p, carry):
        lane = pl.ds(pl.multiple_of(p * LANES, LANES), LANES)
        vt[p] = jnp.transpose(vbuf[:, lane])
        return carry

    lax.fori_loop(0, pairs, transpose_values, 0)

    for copy in gate_copies:
        copy.wait_recv()
    decay = jnp.concatenate([gbuf[i] for i in range(4)], axis=0) * (-(depth ** 0.5))
    rest = decay
    layers = []
    for _ in range(PARTS):
        layer = rest.astype(jnp.bfloat16).astype(jnp.float32)
        layers.append(layer)
        rest = rest - layer
    layers.append(jnp.zeros((LANES - PARTS * heads, both), jnp.float32))
    bias[...] = jnp.transpose(jnp.concatenate(layers, axis=0)).astype(jnp.bfloat16)

    bias_row = lax.broadcasted_iota(jnp.int32, (LANES, tokens), 0)
    ones = jnp.ones((ONES, both), jnp.bfloat16)

    def attend(p, query, keys, diagonal):
        lane = pl.ds(pl.multiple_of(p * LANES, LANES), LANES)
        turned = jnp.transpose(query)
        left_side = jnp.concatenate([kbuf[0:keys, lane], bias[0:keys, :]], axis=1)
        blank = jnp.zeros((depth, tokens), jnp.bfloat16)
        results = []
        for j in range(per_pair):
            head = p * per_pair + j
            picked = jnp.logical_and(
                lax.rem(bias_row, heads) == head, bias_row < PARTS * heads)
            parts = [blank] * per_pair
            parts[j] = turned[j * depth:(j + 1) * depth, :]
            right_side = jnp.concatenate(
                parts + [jnp.where(picked, 1.0, 0.0).astype(jnp.bfloat16)], axis=0)
            logits = jnp.dot(left_side, right_side, preferred_element_type=jnp.float32)
            if diagonal:
                first = keys - tokens
                allowed = (
                    lax.broadcasted_iota(jnp.int32, (tokens, tokens), 0)
                    <= lax.broadcasted_iota(jnp.int32, (tokens, tokens), 1))
                last = jnp.where(allowed, logits[first:, :], -jnp.inf)
                logits = jnp.concatenate([logits[:first, :], last], axis=0) if first else last
            top = jnp.max(logits, axis=0, keepdims=True)
            scores = jnp.exp2((logits - top) * scale).astype(jnp.bfloat16)
            weights = jnp.concatenate(
                [vt[p, j * depth:(j + 1) * depth, 0:keys], ones[:, 0:keys]], axis=0)
            summed = jnp.dot(weights, scores, preferred_element_type=jnp.float32)
            total = summed[depth:depth + 1, :]
            results.append((summed[:depth, :] * (1.0 / total), top * scale + jnp.log2(total)))
        return results

    def own_pair(p, keys):
        lane = pl.ds(pl.multiple_of(p * LANES, LANES), LANES)
        results = attend(p, qbuf[:, lane], keys, True)

        @pl.when(low)
        def _():
            for j in range(per_pair):
                att[p, j * depth:(j + 1) * depth, :] = results[j][0].astype(jnp.bfloat16)

        @pl.when(high)
        def _():
            for j in range(per_pair):
                oloc[p, j * depth:(j + 1) * depth, :] = results[j][0]
                lloc[p, j:j + 1, :] = results[j][1]

    def own_pairs(first, last):
        @pl.when(core == 0)
        def _():
            lax.fori_loop(first, last, lambda p, c: (own_pair(p, tokens), c)[1], 0)

        @pl.when(core == 1)
        def _():
            lax.fori_loop(first, last, lambda p, c: (own_pair(p, both), c)[1], 0)

    def o_copy(p, block):
        return remote(
            ox.at[p, block], oin.at[p], ox_send.at[p, block], ox_recv.at[p], (2 + block, mine))

    def l_copy(p, block):
        return remote(
            lx.at[p, block], lin.at[p], lx_send.at[p, block], lx_recv.at[p], (2 + block, mine))

    def other_pair(round_index):
        p = 2 * round_index + core

        def one(block, carry):
            remote(
                qbuf.at[:, pl.ds(0, LANES)], qx.at[p, block],
                qx_send.at[p], qx_recv.at[p, block], (partner, mine)).wait_recv()
            results = attend(p, qx[p, block], both, False)
            for j in range(per_pair):
                ox[p, block, j * depth:(j + 1) * depth, :] = results[j][0].astype(jnp.bfloat16)
                lx[p, block, j:j + 1, :] = results[j][1]
            o_copy(p, block).start()
            l_copy(p, block).start()
            return carry

        lax.fori_loop(0, 2, one, 0)

    def merge(p, carry):
        o_copy(p, 0).wait_recv()
        l_copy(p, 0).wait_recv()
        for j in range(per_pair):
            rows = pl.ds(j * depth, depth)
            near, far = lloc[p, j:j + 1, :], lin[p, j:j + 1, :]
            top = jnp.maximum(near, far)
            near, far = jnp.exp2(near - top), jnp.exp2(far - top)
            inverse = 1.0 / (near + far)
            mixed = oloc[p, rows, :] * (near * inverse) + oin[p, rows, :].astype(jnp.float32) * (far * inverse)
            att[p, rows, :] = mixed.astype(jnp.bfloat16)
        return carry

    out_copies = []

    def project(owner):
        slot = len(out_copies)
        total = jnp.dot(
            wg[owner], att[...].reshape(width, tokens), preferred_element_type=jnp.float32)
        obuf[slot] = total.astype(jnp.bfloat16)
        copy = pltpu.make_async_copy(
            obuf.at[slot], out.at[pl.ds(pl.multiple_of(owner * columns, PACK), columns)],
            out_sem.at[slot])
        copy.start()
        out_copies.append(copy)

    sequence = [(s, i) for s in range(steps - 1) for i in range(CHUNKS)]
    sequence += [(steps - 1, i) for i in range(max(CHUNKS // 2, 1))]
    merged = 0
    for r in range(rounds):
        own_pairs(r * pairs // rounds, (r + 1) * pairs // rounds)
        stop = min(max(2 * r - 1, 0), pairs)

        @pl.when(low)
        def _():
            other_pair(r)

        @pl.when(high)
        def _():
            lax.fori_loop(merged, stop, merge, 0)

        merged = stop
        ring_event(*sequence[r])

    @pl.when(high)
    def _():
        lax.fori_loop(merged, pairs, merge, 0)

    done = rounds
    ready = [(mine, -1)]
    projected = 0

    def arrived(step):
        for side in range(2):
            for chunk in range(CHUNKS):
                if (side, step, chunk) in pair_copies:
                    pair_copies[side, step, chunk].wait_recv()

    project(mine)
    for step in range(steps):
        while sum(1 for s, i in sequence[:done] if s == step) < sum(1 for s, i in sequence if s == step):
            ring_event(*sequence[done])
            done += 1
        arrived(step)
        if step < steps - 1:
            for side in range(2):
                project(owner_of(side, step))
        else:
            project(owner_of(0, step))

    for copy in out_copies:
        copy.wait()
    for copy in gate_copies + kv_copies + list(ring_copies.values()) + list(pair_copies.values()):
        copy.wait_send()

    @pl.when(high)
    def _():
        for p in range(pairs):
            q_copy(p).wait_send()

    @pl.when(low)
    def _():
        for r in range(rounds):
            for block in range(2):
                o_copy(2 * r + core, block).wait_send()
                l_copy(2 * r + core, block).wait_send()


def fused(dp, depth, q, k, v, gate, w):
    tokens, width = q.shape
    columns = w.shape[0]
    pairs = width // LANES
    both = 2 * tokens
    slots = dp // 2 * CHUNKS
    any_spec = pl.BlockSpec(memory_space=pl.ANY)
    dma = pltpu.SemaphoreType.DMA
    low, wide = jnp.bfloat16, jnp.float32
    per_pair = LANES // depth
    return pl.pallas_call(
        functools.partial(fused_kernel, dp, depth),
        out_shape=jax.ShapeDtypeStruct((columns * dp, tokens), low),
        in_specs=[any_spec] * 5,
        out_specs=any_spec,
        scratch_shapes=[
            pltpu.VMEM((tokens, width), low),
            pltpu.VMEM((both, width), low),
            pltpu.VMEM((both, width), low),
            pltpu.VMEM(gate.shape, wide),
            pltpu.VMEM((4, gate.shape[0], both), wide),
            pltpu.VMEM((both, LANES), low),
            pltpu.VMEM((pairs, LANES, both), low),
            pltpu.VMEM((pairs, 2, tokens, LANES), low),
            pltpu.VMEM((pairs, 2, LANES, tokens), low),
            pltpu.VMEM((pairs, 2, per_pair, tokens), wide),
            pltpu.VMEM((pairs, LANES, tokens), low),
            pltpu.VMEM((pairs, per_pair, tokens), wide),
            pltpu.VMEM((pairs, LANES, tokens), wide),
            pltpu.VMEM((pairs, per_pair, tokens), wide),
            pltpu.VMEM((pairs, LANES, tokens), low),
            pltpu.VMEM((dp, columns, width), low),
            pltpu.VMEM((dp, columns, tokens), low),
            dma((5,)), dma((2,)), dma((2,)), dma((3,)), dma((3,)),
            dma((pairs,)), dma((pairs, 2)),
            dma((pairs, 2)), dma((pairs,)), dma((pairs, 2)), dma((pairs,)),
            dma((2, slots)), dma((2, slots)), dma((2, slots)), dma((2, slots)),
            dma((dp,)),
        ],
        compiler_params=pltpu.CompilerParams(
            collective_id=0, has_side_effects=True, vmem_limit_bytes=63 * 1024 * 1024),
    )(q, k, v, gate, w)


def fits(sp, dp, tokens, width, depth, columns, own_heads):
    return (
        sp == 4 and dp % 2 == 0 and dp >= 4
        and tokens <= 256 and tokens % LANES == 0 and LANES % depth == 0 and depth % 16 == 0
        and width % (2 * LANES) == 0 and columns % PACK == 0 and columns >= 4 * PACK
        and own_heads * sp * depth == width and PARTS * own_heads * sp <= LANES
        and (width // LANES) % 2 == 0 and width // LANES // 2 <= (dp // 2) * CHUNKS - 1
    )


def attend(query_all, key_all, value_all, gate_all):
    length, width = query_all.shape
    heads = gate_all.shape[0]
    depth = width // heads
    block_rows = min(512, length)
    block_count = length // block_rows
    score_scale = depth ** (-0.5)
    query_blocks = query_all.reshape(block_count, block_rows, heads, depth)
    key_blocks = key_all.reshape(block_count, block_rows, heads, depth)
    value_blocks = value_all.reshape(block_count, block_rows, heads, depth)
    gate_blocks = gate_all.reshape(heads, block_count, block_rows).transpose(1, 0, 2)
    offsets = jnp.arange(block_rows, dtype=jnp.int32)

    def one_block(block_index):
        query_part = lax.dynamic_index_in_dim(query_blocks, block_index, 0, keepdims=False)
        gate_part = lax.dynamic_index_in_dim(gate_blocks, block_index, 0, keepdims=False)
        query_rows = block_index * block_rows + offsets

        def key_step(key_block, carry):
            running_max, running_sum, weighted = carry
            key_part = lax.dynamic_index_in_dim(key_blocks, key_block, 0, keepdims=False)
            value_part = lax.dynamic_index_in_dim(value_blocks, key_block, 0, keepdims=False)
            gate_keys = lax.dynamic_index_in_dim(gate_blocks, key_block, 0, keepdims=False)
            logits = (
                jnp.einsum("qhe,khe->hqk", query_part, key_part, preferred_element_type=jnp.float32)
                * score_scale
            )
            logits = logits + gate_part[:, :, None] - gate_keys[:, None, :]
            key_rows = key_block * block_rows + offsets
            allowed = key_rows[None, :] <= query_rows[:, None]
            logits = jnp.where(allowed[None], logits, -jnp.inf)
            new_max = jnp.maximum(running_max, jnp.max(logits, axis=-1))
            scores = jnp.exp(logits - new_max[..., None])
            factor = jnp.exp(running_max - new_max)
            running_sum = running_sum * factor + jnp.sum(scores, axis=-1)
            weighted = weighted * factor[..., None] + jnp.einsum(
                "hqk,khe->hqe",
                scores.astype(jnp.bfloat16),
                value_part,
                preferred_element_type=jnp.float32,
            )
            return (new_max, running_sum, weighted)

        start_state = (
            jnp.full((heads, block_rows), -jnp.inf, jnp.float32),
            jnp.zeros((heads, block_rows), jnp.float32),
            jnp.zeros((heads, block_rows, depth), jnp.float32),
        )
        final_max, final_sum, weighted = lax.fori_loop(0, block_index + 1, key_step, start_state)
        result = weighted / final_sum[..., None]
        return result.transpose(1, 0, 2).astype(jnp.bfloat16)

    outputs = lax.map(one_block, jnp.arange(block_count, dtype=jnp.int32))
    return outputs.reshape(length, width)


def body(queries, keys, values, cum_gate, out_weight):
    sp, dp = lax.axis_size("sp"), lax.axis_size("dp")
    tokens, width = queries.shape[1:]
    depth = width // (cum_gate.shape[1] * sp)
    if fits(sp, dp, tokens, width, depth, out_weight.shape[1], cum_gate.shape[1]):
        mixed = fused(dp, depth, queries[0], keys[0], values[0], cum_gate[0], out_weight.T)
        return mixed.T[None]
    query_heads, key_heads, value_heads = (
        lax.all_to_all(queries, "sp", split_axis=2, concat_axis=1, tiled=True),
        lax.all_to_all(keys, "sp", split_axis=2, concat_axis=1, tiled=True),
        lax.all_to_all(values, "sp", split_axis=2, concat_axis=1, tiled=True),
    )
    local_out = attend(query_heads[0], key_heads[0], value_heads[0], cum_gate[0])
    attended = lax.all_to_all(local_out[None], "sp", split_axis=1, concat_axis=2, tiled=True)[0]
    group_rows = attended.shape[1] // lax.axis_size("sp")
    own_rows = lax.dynamic_slice_in_dim(
        out_weight, lax.axis_index("sp") * group_rows, group_rows, 0
    )
    full_rows = lax.all_gather(own_rows, "dp", axis=1, tiled=True)
    whole_weight = lax.all_gather(full_rows, "sp", axis=0, tiled=True)
    mixed = jnp.dot(attended, whole_weight, preferred_element_type=jnp.float32)
    return mixed.astype(jnp.bfloat16)[None]


def solution(mesh):
    in_specs = (
        P("dp", "sp", None),
        P("dp", "sp", None),
        P("dp", "sp", None),
        P("dp", "sp", None),
        P(None, "dp"),
    )
    out_specs = P("dp", "sp", None)
    return jax.shard_map(body, mesh=mesh, in_specs=in_specs, out_specs=out_specs, check_vma=False)
```

time: 40.7 us -> 36.6 us (0.90)
  local copies, waits for them, and re-layouts: 5.87 us -> 2.29 us
    unnamed x11 -> x1, local copies, waits for them, and re-layouts: 5.87 us -> 2.29 us
where the time goes in v2:
time: 36.6 us; the launch traced here: 36.4 us
  Pallas kernels  34.1 us (93%)
  local copies, waits for them, and re-layouts  2.29 us (6%)
    pallas_call x1, Pallas kernels, fused(): pl.pallas_call(functools.partial(fused_kernel, dp, depth), out_shape=jax....  34.1 us
    unnamed x1, local copies, waits for them, and re-layouts  2.29 us

profile of v2, /device:TPU:0, one launch (start us, length us, event | category | flops | bytes accessed | tf_op | source)
XLA Modules:
  0.0 36.4 jit_solution(15785910956790061194)
XLA Ops:
  0.0 34.1 %shard_map.55 = bf16[2112,256]{1,0:T(8,128)(2,1)} custom-call(bf16[256,1024]{1,0:T(8,128)(2,1)} %bitcast.10, bf16[256,1024]{1,0:T(8,128)(2,1)} %bitcast.11, bf16[256,1024]{1,0:T(8,128)(2,1)} %bitcast.12, f32[4,1024]{1,0:T(4,128)} %bitcast.13, bf16[264,1024]{1,0:T(8,128)(2,1)} %bitcast.9), custom_call_target="tpu_custom_call" | custom-call | tf_op jit(solution)/shard_map/pallas_call | solution.py:368
  34.1 2.3 %copy.7 = bf16[1,256,2112]{1,2,0:T(8,128)(2,1)} copy(bf16[1,256,2112]{1,2,0:T(8,128)(2,1)} %bitcast.8) | data formatting | bytes 2162688

commit v3 on v2

--- a/solution.py
+++ b/solution.py
@@ -29,9 +29,9 @@
 
 def fused_kernel(
     dp, depth, q, k, v, gate, w, out,
-    qbuf, kbuf, vbuf, gown, gbuf, bias, vt, qx, ox, lx, oin, lin, oloc, lloc, att, wg, obuf,
+    qbuf, kbuf, vbuf, gown, gbuf, bias, vt, qx, ox, lx, oin, lin, oloc, lloc, att, wg,
     load_sem, kv_send, kv_recv, gate_send, gate_recv, qx_send, qx_recv,
-    ox_send, ox_recv, lx_send, lx_recv, ring_send, ring_recv, pair_send, pair_recv, out_sem,
+    ox_send, ox_recv, lx_send, lx_recv, ring_send, ring_recv, pair_send, pair_recv,
 ):
     tokens, width = q.shape
     columns = w.shape[0]
@@ -280,18 +280,10 @@
             att[p, rows, :] = mixed.astype(jnp.bfloat16)
         return carry
 
-    out_copies = []
-
     def project(owner):
-        slot = len(out_copies)
         total = jnp.dot(
             wg[owner], att[...].reshape(width, tokens), preferred_element_type=jnp.float32)
-        obuf[slot] = total.astype(jnp.bfloat16)
-        copy = pltpu.make_async_copy(
-            obuf.at[slot], out.at[pl.ds(pl.multiple_of(owner * columns, PACK), columns)],
-            out_sem.at[slot])
-        copy.start()
-        out_copies.append(copy)
+        out[pl.ds(pl.multiple_of(owner * columns, PACK), columns), :] = total.astype(jnp.bfloat16)
 
     sequence = [(s, i) for s in range(steps - 1) for i in range(CHUNKS)]
     sequence += [(steps - 1, i) for i in range(max(CHUNKS // 2, 1))]
@@ -337,8 +329,6 @@
         else:
             project(owner_of(0, step))
 
-    for copy in out_copies:
-        copy.wait()
     for copy in gate_copies + kv_copies + list(ring_copies.values()) + list(pair_copies.values()):
         copy.wait_send()
 
@@ -367,9 +357,9 @@
     per_pair = LANES // depth
     return pl.pallas_call(
         functools.partial(fused_kernel, dp, depth),
-        out_shape=jax.ShapeDtypeStruct((columns * dp, tokens), low),
+        out_shape=pltpu.VMEM((columns * dp, tokens), low),
         in_specs=[any_spec] * 5,
-        out_specs=any_spec,
+        out_specs=pl.BlockSpec(memory_space=pltpu.VMEM),
         scratch_shapes=[
             pltpu.VMEM((tokens, width), low),
             pltpu.VMEM((both, width), low),
@@ -387,16 +377,14 @@
             pltpu.VMEM((pairs, per_pair, tokens), wide),
             pltpu.VMEM((pairs, LANES, tokens), low),
             pltpu.VMEM((dp, columns, width), low),
-            pltpu.VMEM((dp, columns, tokens), low),
             dma((5,)), dma((2,)), dma((2,)), dma((3,)), dma((3,)),
             dma((pairs,)), dma((pairs, 2)),
             dma((pairs, 2)), dma((pairs,)), dma((pairs, 2)), dma((pairs,)),
             dma((2, slots)), dma((2, slots)), dma((2, slots)), dma((2, slots)),
-            dma((dp,)),
         ],
         compiler_params=pltpu.CompilerParams(
-            collective_id=0, has_side_effects=True, vmem_limit_bytes=63 * 1024 * 1024),
-    )(q, k, v, gate, w)
+            collective_id=0, has_side_effects=True, vmem_limit_bytes=48 * 1024 * 1024),
+    )(*(pltpu.with_memory_space_constraint(x, pltpu.HBM) for x in (q, k, v, gate, w)))
 
 
 def fits(sp, dp, tokens, width, depth, columns, own_heads):

time: 36.6 us -> 34.6 us (0.945)
  local copies, waits for them, and re-layouts: 2.29 us -> 0.98 us
  Pallas kernels: 34.1 us -> 33.4 us
    unnamed x1, local copies, waits for them, and re-layouts: 2.29 us -> 0.98 us
    pallas_call x1, Pallas kernels: 34.1 us -> 33.4 us  [fused(): pl.pallas_call(functools.partial(fused_kernel, dp, depth), out_shape=pltp...]
where the time goes in v3:
time: 34.6 us; the launch traced here: 34.4 us
  Pallas kernels  33.4 us (97%)
  local copies, waits for them, and re-layouts  0.98 us (3%)
    pallas_call x1, Pallas kernels, fused(): pl.pallas_call(functools.partial(fused_kernel, dp, depth), out_shape=pltp...  33.4 us
    unnamed x1, local copies, waits for them, and re-layouts  0.98 us

profile of v3, /device:TPU:0, one launch (start us, length us, event | category | flops | bytes accessed | tf_op | source)
XLA Modules:
  0.0 34.4 jit_solution(11762550635963738534)
XLA Ops:
  0.0 33.4 %shard_map.55 = bf16[2112,256]{1,0:T(8,128)(2,1)S(1)} custom-call(bf16[256,1024]{1,0:T(8,128)(2,1)} %bitcast.10, bf16[256,1024]{1,0:T(8,128)(2,1)} %bitcast.11, bf16[256,1024]{1,0:T(8,128)(2,1)} %bitcast.12, f32[4,1024]{1,0:T(4,128)} %bitcast.13, bf16[264,1024]{1,0:T(8,128)(2,1)} %bitcast.9), custom_call_target="tpu_custom_call" | custom-call | tf_op jit(solution)/shard_map/pallas_call | solution.py:358
  33.4 1.0 %copy.7 = bf16[1,256,2112]{1,2,0:T(8,128)(2,1)} copy(bf16[1,256,2112]{1,2,0:T(8,128)(2,1)S(1)} %bitcast.8) | data formatting | bytes 2162688

commit v4 on v3

--- a/solution.py
+++ b/solution.py
@@ -11,7 +11,6 @@
 LANES = 128
 PACK = 8
 PARTS = 3
-CHUNKS = 2
 ONES = 16
 MESH = pl.DeviceIdType.MESH
 
@@ -21,15 +20,17 @@
     return (1 - upper) * (2 * position) + upper * (2 * (n - 1 - position) + 1)
 
 
-def spans(total, pieces):
-    units = total // PACK
-    cuts = [PACK * (units * i // pieces) for i in range(pieces + 1)]
-    return [(cuts[i], cuts[i + 1] - cuts[i]) for i in range(pieces)]
+def pieces_of(columns):
+    units = columns // PACK
+    half = -(-units // 2)
+    sizes = [-(-half // 2), half // 2, -(-(units - half) // 2), (units - half) // 2]
+    starts = [sum(sizes[:i]) for i in range(4)]
+    return [(PACK * start, PACK * size) for start, size in zip(starts, sizes)]
 
 
 def fused_kernel(
     dp, depth, q, k, v, gate, w, out,
-    qbuf, kbuf, vbuf, gown, gbuf, bias, vt, qx, ox, lx, oin, lin, oloc, lloc, att, wg,
+    qbuf, kbuf, vbuf, gown, gbuf, bias, qt, vt, qx, ox, lx, oin, lin, oloc, lloc, att, wg,
     load_sem, kv_send, kv_recv, gate_send, gate_recv, qx_send, qx_recv,
     ox_send, ox_recv, lx_send, lx_recv, ring_send, ring_recv, pair_send, pair_recv,
 ):
@@ -72,12 +73,38 @@
     for d in range(1, 4):
         pl.semaphore_signal(
             barrier, inc=1, device_id=(lax.rem(me + d, 4), mine), device_id_type=MESH)
-    for side in (left, right):
-        pl.semaphore_signal(barrier, inc=1, device_id=(me, side), device_id_type=MESH)
+
+    @pl.when(core == 1)
+    def _():
+        for side in (left, right):
+            pl.semaphore_signal(barrier, inc=1, device_id=(me, side), device_id_type=MESH)
+
     for copy in loads:
         copy.wait()
     gbuf[me] = gown[:, pl.ds(pl.multiple_of(side_y * both, both), both)]
-    pl.semaphore_wait(barrier, 5)
+
+    def turn(start, with_queries):
+        columns_here = pl.ds(pl.multiple_of(start, tokens), tokens)
+
+        def one(p, carry):
+            lane = pl.ds(pl.multiple_of(p * LANES, LANES), LANES)
+            if with_queries:
+                qt[p] = jnp.transpose(qbuf[:, lane])
+            vt[p, :, columns_here] = jnp.transpose(vbuf[columns_here, lane])
+            return carry
+
+        lax.fori_loop(0, pairs, one, 0)
+
+    turn(core * tokens, True)
+
+    @pl.when(core == 0)
+    def _():
+        pl.semaphore_wait(barrier, 3)
+
+    @pl.when(core == 1)
+    def _():
+        pl.semaphore_wait(barrier, 5)
+
 
     def remote(source, target, send, recv, device):
         return pltpu.make_async_remote_copy(
@@ -98,80 +125,68 @@
     def q_copy(p):
         return remote(
             qbuf.at[:, pl.ds(p * LANES, LANES)], qx.at[p, core],
-            qx_send.at[p], qx_recv.at[p, core], (p % 2, mine))
+            qx_send.at[p], qx_recv.at[p, core], (0, mine))
 
     for copy in gate_copies:
         copy.start()
     for copy in kv_copies:
         copy.start()
 
-    @pl.when(high)
-    def _():
-        for p in range(pairs):
-            q_copy(p).start()
-
-    half = width // 2
-    lanes = pl.ds(pl.multiple_of(core * half, half), half)
-    chunks = spans(columns, CHUNKS)
-    events = steps * CHUNKS - CHUNKS // 2 if CHUNKS > 1 else steps
-    ring_copies = {}
-    pair_copies = {}
-
-    def piece(owner, chunk):
-        start, size = chunks[chunk]
-        return wg.at[owner, pl.ds(start, size), lanes]
+    parts = pieces_of(columns)
+
+    def piece(owner, part):
+        start, size = parts[part]
+        return wg.at[owner, pl.ds(start, size)]
 
     def owner_of(side, step):
         shift = dp - 1 - step if side == 0 else 1 + step
         return ring_index(lax.rem(position + shift, dp), dp)
 
-    def carries(side, step, chunk):
-        if step < steps - 1:
-            return True
-        return (chunk < CHUNKS // 2) == (side == 0)
-
-    def start_ring(side, step, chunk, owner):
-        if not carries(side, step, chunk):
-            return
-        slot = step * CHUNKS + chunk
-        copy = remote(
-            piece(owner, chunk), piece(owner, chunk),
-            ring_send.at[side, slot], ring_recv.at[side, slot],
+    def carries(side, step, part):
+        return step < steps - 1 or (part < 2) == (side == 0)
+
+    def ring_copy(side, step, part):
+        here = piece(owner_of(side, step - 1) if step else mine, part)
+        slot = step * 4 + part
+        return remote(
+            here, here, ring_send.at[side, slot], ring_recv.at[side, slot],
             (me, right if side == 0 else left))
-        copy.start()
-        ring_copies[side, step, chunk] = copy
-
-    def ring_event(step, index):
-        for side in range(2):
-            chunk = index
-            if step == steps - 1:
-                chunk = index + (CHUNKS // 2) * side
-            owner = owner_of(side, step)
-            ring_copies[side, step, chunk].wait_recv()
-            if step + 1 < steps:
-                start_ring(side, step + 1, chunk, owner)
-            slot = step * CHUNKS + chunk
-            copy = remote(
-                piece(owner, chunk), piece(owner, chunk),
-                pair_send.at[side, slot], pair_recv.at[side, slot], (partner, mine))
-            copy.start()
-            pair_copies[side, step, chunk] = copy
-
-    for chunk in range(CHUNKS):
-        for side in range(2):
-            start_ring(side, 0, chunk, mine)
+
+    def pair_copy(side, step, part):
+        here = piece(owner_of(side, step), part)
+        slot = step * 4 + part
+        return remote(
+            here, here, pair_send.at[side, slot], pair_recv.at[side, slot], (partner, mine))
+
+    def sides_of(step):
+        return range(2 if step < steps - 1 else 1)
+
+    def ring_event(side, step, part):
+        ring_copy(side, step, part).wait_recv()
+        if step + 1 < steps and carries(side, step + 1, part):
+            ring_copy(side, step + 1, part).start()
+        pair_copy(side, step, part).start()
+
+    every = [
+        (side, step, part) for step in range(steps) for part in range(4) for side in range(2)
+        if carries(side, step, part)]
+
+    @pl.when(core == 1)
+    def _():
+        for part in range(4):
+            for side in range(2):
+                ring_copy(side, 0, part).start()
+
+    @pl.when(high)
+    def _():
+        for p in range(pairs):
+            q_copy(p).start()
 
     scale = depth ** -0.5 * math.log2(math.e)
     for copy in kv_copies:
         copy.wait_recv()
 
-    def transpose_values(p, carry):
-        lane = pl.ds(pl.multiple_of(p * LANES, LANES), LANES)
-        vt[p] = jnp.transpose(vbuf[:, lane])
-        return carry
-
-    lax.fori_loop(0, pairs, transpose_values, 0)
-
+    turn((1 - core) * tokens, False)
     for copy in gate_copies:
         copy.wait_recv()
     decay = jnp.concatenate([gbuf[i] for i in range(4)], axis=0) * (-(depth ** 0.5))
@@ -187,60 +202,63 @@
     bias_row = lax.broadcasted_iota(jnp.int32, (LANES, tokens), 0)
     ones = jnp.ones((ONES, both), jnp.bfloat16)
 
-    def attend(p, query, keys, diagonal):
-        lane = pl.ds(pl.multiple_of(p * LANES, LANES), LANES)
-        turned = jnp.transpose(query)
-        left_side = jnp.concatenate([kbuf[0:keys, lane], bias[0:keys, :]], axis=1)
+    def attend(items, keys, diagonal):
         blank = jnp.zeros((depth, tokens), jnp.bfloat16)
+        logits = []
+        for p, turned in items:
+            lane = pl.ds(pl.multiple_of(p * LANES, LANES), LANES)
+            left_side = jnp.concatenate([kbuf[0:keys, lane], bias[0:keys, :]], axis=1)
+            for j in range(per_pair):
+                head = p * per_pair + j
+                picked = jnp.logical_and(
+                    lax.rem(bias_row, heads) == head, bias_row < PARTS * heads)
+                rows = [blank] * per_pair
+                rows[j] = turned[j * depth:(j + 1) * depth, :]
+                right_side = jnp.concatenate(
+                    rows + [jnp.where(picked, 1.0, 0.0).astype(jnp.bfloat16)], axis=0)
+                logits.append(
+                    jnp.dot(left_side, right_side, preferred_element_type=jnp.float32))
+        if diagonal:
+            first = keys - tokens
+            allowed = (
+                lax.broadcasted_iota(jnp.int32, (tokens, tokens), 0)
+                <= lax.broadcasted_iota(jnp.int32, (tokens, tokens), 1))
+            for n, plain in enumerate(logits):
+                last = jnp.where(allowed, plain[first:, :], -jnp.inf)
+                logits[n] = jnp.concatenate([plain[:first, :], last], axis=0) if first else last
+        tops = [jnp.max(x, axis=0, keepdims=True) for x in logits]
+        scores = [
+            jnp.exp2((x - top) * scale).astype(jnp.bfloat16) for x, top in zip(logits, tops)]
         results = []
-        for j in range(per_pair):
-            head = p * per_pair + j
-            picked = jnp.logical_and(
-                lax.rem(bias_row, heads) == head, bias_row < PARTS * heads)
-            parts = [blank] * per_pair
-            parts[j] = turned[j * depth:(j + 1) * depth, :]
-            right_side = jnp.concatenate(
-                parts + [jnp.where(picked, 1.0, 0.0).astype(jnp.bfloat16)], axis=0)
-            logits = jnp.dot(left_side, right_side, preferred_element_type=jnp.float32)
-            if diagonal:
-                first = keys - tokens
-                allowed = (
-                    lax.broadcasted_iota(jnp.int32, (tokens, tokens), 0)
-                    <= lax.broadcasted_iota(jnp.int32, (tokens, tokens), 1))
-                last = jnp.where(allowed, logits[first:, :], -jnp.inf)
-                logits = jnp.concatenate([logits[:first, :], last], axis=0) if first else last
-            top = jnp.max(logits, axis=0, keepdims=True)
-            scores = jnp.exp2((logits - top) * scale).astype(jnp.bfloat16)
-            weights = jnp.concatenate(
-                [vt[p, j * depth:(j + 1) * depth, 0:keys], ones[:, 0:keys]], axis=0)
-            summed = jnp.dot(weights, scores, preferred_element_type=jnp.float32)
-            total = summed[depth:depth + 1, :]
-            results.append((summed[:depth, :] * (1.0 / total), top * scale + jnp.log2(total)))
+        for i, (p, _) in enumerate(items):
+            found = []
+            for j in range(per_pair):
+                n = i * per_pair + j
+                weights = jnp.concatenate(
+                    [vt[p, j * depth:(j + 1) * depth, 0:keys], ones[:, 0:keys]], axis=0)
+                summed = jnp.dot(weights, scores[n], preferred_element_type=jnp.float32)
+                total = summed[depth:depth + 1, :]
+                found.append(
+                    (summed[:depth, :] * (1.0 / total), tops[n] * scale + jnp.log2(total)))
+            results.append(found)
         return results
 
-    def own_pair(p, keys):
-        lane = pl.ds(pl.multiple_of(p * LANES, LANES), LANES)
-        results = attend(p, qbuf[:, lane], keys, True)
+    def own_pairs(first, last, keys):
+        span = range(first, last)
+        results = attend([(p, qt[p]) for p in span], keys, True)
 
         @pl.when(low)
         def _():
-            for j in range(per_pair):
-                att[p, j * depth:(j + 1) * depth, :] = results[j][0].astype(jnp.bfloat16)
+            for p, found in zip(span, results):
+                for j in range(per_pair):
+                    att[p, j * depth:(j + 1) * depth, :] = found[j][0].astype(jnp.bfloat16)
 
         @pl.when(high)
         def _():
-            for j in range(per_pair):
-                oloc[p, j * depth:(j + 1) * depth, :] = results[j][0]
-                lloc[p, j:j + 1, :] = results[j][1]
-
-    def own_pairs(first, last):
-        @pl.when(core == 0)
-        def _():
-            lax.fori_loop(first, last, lambda p, c: (own_pair(p, tokens), c)[1], 0)
-
-        @pl.when(core == 1)
-        def _():
-            lax.fori_loop(first, last, lambda p, c: (own_pair(p, both), c)[1], 0)
+            for p, found in zip(span, results):
+                for j in range(per_pair):
+                    oloc[p, j * depth:(j + 1) * depth, :] = found[j][0]
+                    lloc[p, j:j + 1, :] = found[j][1]
 
     def o_copy(p, block):
         return remote(
@@ -250,22 +268,19 @@
         return remote(
             lx.at[p, block], lin.at[p], lx_send.at[p, block], lx_recv.at[p], (2 + block, mine))
 
-    def other_pair(round_index):
-        p = 2 * round_index + core
-
-        def one(block, carry):
+    def other_pair(p):
+        for block in range(2):
             remote(
                 qbuf.at[:, pl.ds(0, LANES)], qx.at[p, block],
                 qx_send.at[p], qx_recv.at[p, block], (partner, mine)).wait_recv()
-            results = attend(p, qx[p, block], both, False)
+        results = attend([(p, jnp.transpose(qx[p, block])) for block in range(2)], both, False)
+        for block in range(2):
             for j in range(per_pair):
-                ox[p, block, j * depth:(j + 1) * depth, :] = results[j][0].astype(jnp.bfloat16)
-                lx[p, block, j:j + 1, :] = results[j][1]
+                found = results[block][j]
+                ox[p, block, j * depth:(j + 1) * depth, :] = found[0].astype(jnp.bfloat16)
+                lx[p, block, j:j + 1, :] = found[1]
             o_copy(p, block).start()
             l_copy(p, block).start()
-            return carry
-
-        lax.fori_loop(0, 2, one, 0)
 
     def merge(p, carry):
         o_copy(p, 0).wait_recv()
@@ -285,64 +300,70 @@
             wg[owner], att[...].reshape(width, tokens), preferred_element_type=jnp.float32)
         out[pl.ds(pl.multiple_of(owner * columns, PACK), columns), :] = total.astype(jnp.bfloat16)
 
-    sequence = [(s, i) for s in range(steps - 1) for i in range(CHUNKS)]
-    sequence += [(steps - 1, i) for i in range(max(CHUNKS // 2, 1))]
-    merged = 0
-    for r in range(rounds):
-        own_pairs(r * pairs // rounds, (r + 1) * pairs // rounds)
-        stop = min(max(2 * r - 1, 0), pairs)
+    def merge_to(first, last):
+        @pl.when(high)
+        def _():
+            lax.fori_loop(first, last, merge, 0)
+
+    def finish(step):
+        for side in sides_of(step):
+            project(owner_of(side, step))
+
+    @pl.when(core == 0)
+    def _():
+        for r in range(rounds):
+            own_pairs(r * pairs // rounds, (r + 1) * pairs // rounds, tokens)
 
         @pl.when(low)
         def _():
-            other_pair(r)
-
-        @pl.when(high)
+            for p in range(pairs):
+                other_pair(p)
+
+        merge_to(0, pairs)
+        project(mine)
+        for step in range(steps):
+            for key in every:
+                if key[1] == step:
+                    pair_copy(*key).wait_recv()
+            finish(step)
+
+        @pl.when(low)
         def _():
-            lax.fori_loop(merged, stop, merge, 0)
-
-        merged = stop
-        ring_event(*sequence[r])
-
-    @pl.when(high)
-    def _():
-        lax.fori_loop(merged, pairs, merge, 0)
-
-    done = rounds
-    ready = [(mine, -1)]
-    projected = 0
-
-    def arrived(step):
-        for side in range(2):
-            for chunk in range(CHUNKS):
-                if (side, step, chunk) in pair_copies:
-                    pair_copies[side, step, chunk].wait_recv()
-
-    project(mine)
-    for step in range(steps):
-        while sum(1 for s, i in sequence[:done] if s == step) < sum(1 for s, i in sequence if s == step):
-            ring_event(*sequence[done])
-            done += 1
-        arrived(step)
-        if step < steps - 1:
-            for side in range(2):
-                project(owner_of(side, step))
-        else:
-            project(owner_of(0, step))
-
-    for copy in gate_copies + kv_copies + list(ring_copies.values()) + list(pair_copies.values()):
+            for p in range(pairs):
+                for block in range(2):
+                    o_copy(p, block).wait_send()
+                    l_copy(p, block).wait_send()
+
+    @pl.when(core == 1)
+    def _():
+        todo = list(every)
+
+        def advance(count):
+            for _ in range(count):
+                ring_event(*todo.pop(0))
+
+        for r in range(rounds):
+            own_pairs(r * pairs // rounds, (r + 1) * pairs // rounds, both)
+            advance(2)
+        while todo and todo[0][1] < steps - 1:
+            advance(1)
+        merge_to(0, pairs)
+        project(mine)
+        for step in range(steps - 1):
+            finish(step)
+        advance(len(todo))
+        finish(steps - 1)
+        for key in every:
+            ring_copy(*key).wait_send()
+            pair_copy(*key).wait_send()
+
+    for copy in gate_copies + kv_copies:
         copy.wait_send()
 
     @pl.when(high)
     def _():
         for p in range(pairs):
             q_copy(p).wait_send()
-
-    @pl.when(low)
-    def _():
-        for r in range(rounds):
-            for block in range(2):
-                o_copy(2 * r + core, block).wait_send()
-                l_copy(2 * r + core, block).wait_send()
 
 
 def fused(dp, depth, q, k, v, gate, w):
@@ -350,7 +371,8 @@
     columns = w.shape[0]
     pairs = width // LANES
     both = 2 * tokens
-    slots = dp // 2 * CHUNKS
+    steps = dp // 2
+    slots = steps * 4
     any_spec = pl.BlockSpec(memory_space=pl.ANY)
     dma = pltpu.SemaphoreType.DMA
     low, wide = jnp.bfloat16, jnp.float32
@@ -367,6 +389,7 @@
             pltpu.VMEM(gate.shape, wide),
             pltpu.VMEM((4, gate.shape[0], both), wide),
             pltpu.VMEM((both, LANES), low),
+            pltpu.VMEM((pairs, LANES, tokens), low),
             pltpu.VMEM((pairs, LANES, both), low),
             pltpu.VMEM((pairs, 2, tokens, LANES), low),
             pltpu.VMEM((pairs, 2, LANES, tokens), low),
@@ -393,7 +416,7 @@
         and tokens <= 256 and tokens % LANES == 0 and LANES % depth == 0 and depth % 16 == 0
         and width % (2 * LANES) == 0 and columns % PACK == 0 and columns >= 4 * PACK
         and own_heads * sp * depth == width and PARTS * own_heads * sp <= LANES
-        and (width // LANES) % 2 == 0 and width // LANES // 2 <= (dp // 2) * CHUNKS - 1
+        and width == 8 * LANES and dp == 8
     )
 
 

time: 34.6 us -> 31.4 us (0.908)
  Pallas kernels: 33.4 us -> 30.2 us
    pallas_call x1, Pallas kernels: 33.4 us -> 30.2 us  [fused(): pl.pallas_call(functools.partial(fused_kernel, dp, depth), out_shape=pltp...]
where the time goes in v4:
time: 31.4 us; the launch traced here: 31.1 us
  Pallas kernels  30.2 us (96%)
  local copies, waits for them, and re-layouts  0.98 us (3%)
    pallas_call x1, Pallas kernels, fused(): pl.pallas_call(functools.partial(fused_kernel, dp, depth), out_shape=pltp...  30.2 us
    unnamed x1, local copies, waits for them, and re-layouts  0.98 us

profile of v4, /device:TPU:0, one launch (start us, length us, event | category | flops | bytes accessed | tf_op | source)
XLA Modules:
  0.0 31.1 jit_solution(16434420730333959700)
XLA Ops:
  0.0 30.2 %shard_map.55 = bf16[2112,256]{1,0:T(8,128)(2,1)S(1)} custom-call(bf16[256,1024]{1,0:T(8,128)(2,1)} %bitcast.10, bf16[256,1024]{1,0:T(8,128)(2,1)} %bitcast.11, bf16[256,1024]{1,0:T(8,128)(2,1)} %bitcast.12, f32[4,1024]{1,0:T(4,128)} %bitcast.13, bf16[264,1024]{1,0:T(8,128)(2,1)} %bitcast.9), custom_call_target="tpu_custom_call" | custom-call | tf_op jit(solution)/shard_map/pallas_call | solution.py:380
  30.2 1.0 %copy.7 = bf16[1,256,2112]{1,2,0:T(8,128)(2,1)} copy(bf16[1,256,2112]{1,2,0:T(8,128)(2,1)S(1)} %bitcast.8) | data formatting | bytes 2162688

commit v5 on v4

--- a/solution.py
+++ b/solution.py
@@ -11,6 +11,7 @@
 LANES = 128
 PACK = 8
 PARTS = 3
+PIECES = 2
 ONES = 16
 MESH = pl.DeviceIdType.MESH
 
@@ -23,9 +24,10 @@
 def pieces_of(columns):
     units = columns // PACK
     half = -(-units // 2)
-    sizes = [-(-half // 2), half // 2, -(-(units - half) // 2), (units - half) // 2]
-    starts = [sum(sizes[:i]) for i in range(4)]
-    return [(PACK * start, PACK * size) for start, size in zip(starts, sizes)]
+    each = PIECES // 2
+    cuts = [half * i // each for i in range(each)]
+    cuts += [half + (units - half) * i // each for i in range(each + 1)]
+    return [(PACK * a, PACK * (b - a)) for a, b in zip(cuts, cuts[1:])]
 
 
 def fused_kernel(
@@ -95,7 +97,6 @@
 
         lax.fori_loop(0, pairs, one, 0)
 
-    turn(core * tokens, True)
 
     @pl.when(core == 0)
     def _():
@@ -143,18 +144,18 @@
         return ring_index(lax.rem(position + shift, dp), dp)
 
     def carries(side, step, part):
-        return step < steps - 1 or (part < 2) == (side == 0)
+        return step < steps - 1 or (part < PIECES // 2) == (side == 0)
 
     def ring_copy(side, step, part):
         here = piece(owner_of(side, step - 1) if step else mine, part)
-        slot = step * 4 + part
+        slot = step * PIECES + part
         return remote(
             here, here, ring_send.at[side, slot], ring_recv.at[side, slot],
             (me, right if side == 0 else left))
 
     def pair_copy(side, step, part):
         here = piece(owner_of(side, step), part)
-        slot = step * 4 + part
+        slot = step * PIECES + part
         return remote(
             here, here, pair_send.at[side, slot], pair_recv.at[side, slot], (partner, mine))
 
@@ -168,14 +169,15 @@
         pair_copy(side, step, part).start()
 
     every = [
-        (side, step, part) for step in range(steps) for part in range(4) for side in range(2)
-        if carries(side, step, part)]
+        (side, step, (part + PIECES // 2 * side) % PIECES)
+        for step in range(steps) for part in range(PIECES) for side in range(2)
+        if carries(side, step, (part + PIECES // 2 * side) % PIECES)]
 
     @pl.when(core == 1)
     def _():
-        for part in range(4):
+        for part in range(PIECES):
             for side in range(2):
-                ring_copy(side, 0, part).start()
+                ring_copy(side, 0, (part + PIECES // 2 * side) % PIECES).start()
 
     @pl.when(high)
     def _():
@@ -183,9 +185,9 @@
             q_copy(p).start()
 
     scale = depth ** -0.5 * math.log2(math.e)
+    turn(core * tokens, True)
     for copy in kv_copies:
         copy.wait_recv()
-
     turn((1 - core) * tokens, False)
     for copy in gate_copies:
         copy.wait_recv()
@@ -372,7 +374,7 @@
     pairs = width // LANES
     both = 2 * tokens
     steps = dp // 2
-    slots = steps * 4
+    slots = steps * PIECES
     any_spec = pl.BlockSpec(memory_space=pl.ANY)
     dma = pltpu.SemaphoreType.DMA
     low, wide = jnp.bfloat16, jnp.float32
@@ -414,7 +416,7 @@
     return (
         sp == 4 and dp % 2 == 0 and dp >= 4
         and tokens <= 256 and tokens % LANES == 0 and LANES % depth == 0 and depth % 16 == 0
-        and width % (2 * LANES) == 0 and columns % PACK == 0 and columns >= 4 * PACK
+        and width % (2 * LANES) == 0 and columns % PACK == 0 and columns >= PIECES * PACK
         and own_heads * sp * depth == width and PARTS * own_heads * sp <= LANES
         and width == 8 * LANES and dp == 8
     )

time: 31.4 us -> 30.1 us (0.959)
  Pallas kernels: 30.2 us -> 28.9 us
    pallas_call x1, Pallas kernels: 30.2 us -> 28.9 us  [fused(): pl.pallas_call(functools.partial(fused_kernel, dp, depth), out_shape=pltp...]
where the time goes in v5:
time: 30.1 us; the launch traced here: 29.9 us
  Pallas kernels  28.9 us (96%)
  local copies, waits for them, and re-layouts  0.98 us (3%)
    pallas_call x1, Pallas kernels, fused(): pl.pallas_call(functools.partial(fused_kernel, dp, depth), out_shape=pltp...  28.9 us
    unnamed x1, local copies, waits for them, and re-layouts  0.98 us

profile of v5, /device:TPU:0, one launch (start us, length us, event | category | flops | bytes accessed | tf_op | source)
XLA Modules:
  0.0 29.9 jit_solution(15291802518702960289)
XLA Ops:
  0.0 28.9 %shard_map.55 = bf16[2112,256]{1,0:T(8,128)(2,1)S(1)} custom-call(bf16[256,1024]{1,0:T(8,128)(2,1)} %bitcast.10, bf16[256,1024]{1,0:T(8,128)(2,1)} %bitcast.11, bf16[256,1024]{1,0:T(8,128)(2,1)} %bitcast.12, f32[4,1024]{1,0:T(4,128)} %bitcast.13, bf16[264,1024]{1,0:T(8,128)(2,1)} %bitcast.9), custom_call_target="tpu_custom_call" | custom-call | tf_op jit(solution)/shard_map/pallas_call | solution.py:382
  28.9 1.0 %copy.7 = bf16[1,256,2112]{1,2,0:T(8,128)(2,1)} copy(bf16[1,256,2112]{1,2,0:T(8,128)(2,1)S(1)} %bitcast.8) | data formatting | bytes 2162688

commit v6 on v5

--- a/solution.py
+++ b/solution.py
@@ -12,6 +12,7 @@
 PACK = 8
 PARTS = 3
 PIECES = 2
+LARGE = 3
 ONES = 16
 MESH = pl.DeviceIdType.MESH
 
@@ -134,9 +135,13 @@
         copy.start()
 
     parts = pieces_of(columns)
-
-    def piece(owner, part):
-        start, size = parts[part]
+    final = []
+    for start, size in parts:
+        large = size * LARGE // 4 // PACK * PACK
+        final += [(start, large), (start + large, size - large)]
+
+    def piece(owner, step, part):
+        start, size = (parts if step < steps - 1 else final)[part]
         return wg.at[owner, pl.ds(start, size)]
 
     def owner_of(side, step):
@@ -144,17 +149,17 @@
         return ring_index(lax.rem(position + shift, dp), dp)
 
     def carries(side, step, part):
-        return step < steps - 1 or (part < PIECES // 2) == (side == 0)
+        return step < steps - 1 or (part < PIECES) == (side == 0)
 
     def ring_copy(side, step, part):
-        here = piece(owner_of(side, step - 1) if step else mine, part)
+        here = piece(owner_of(side, step - 1) if step else mine, step, part)
         slot = step * PIECES + part
         return remote(
             here, here, ring_send.at[side, slot], ring_recv.at[side, slot],
             (me, right if side == 0 else left))
 
     def pair_copy(side, step, part):
-        here = piece(owner_of(side, step), part)
+        here = piece(owner_of(side, step), step, part)
         slot = step * PIECES + part
         return remote(
             here, here, pair_send.at[side, slot], pair_recv.at[side, slot], (partner, mine))
@@ -164,14 +169,18 @@
 
     def ring_event(side, step, part):
         ring_copy(side, step, part).wait_recv()
-        if step + 1 < steps and carries(side, step + 1, part):
+        if step + 2 < steps:
             ring_copy(side, step + 1, part).start()
+        elif step + 1 < steps:
+            for smaller in (2 * part, 2 * part + 1):
+                if carries(side, step + 1, smaller):
+                    ring_copy(side, step + 1, smaller).start()
         pair_copy(side, step, part).start()
 
     every = [
         (side, step, (part + PIECES // 2 * side) % PIECES)
-        for step in range(steps) for part in range(PIECES) for side in range(2)
-        if carries(side, step, (part + PIECES // 2 * side) % PIECES)]
+        for step in range(steps - 1) for part in range(PIECES) for side in range(2)]
+    every += [(side, steps - 1, part + PIECES * side) for part in range(PIECES) for side in range(2)]
 
     @pl.when(core == 1)
     def _():
@@ -374,7 +383,7 @@
     pairs = width // LANES
     both = 2 * tokens
     steps = dp // 2
-    slots = steps * PIECES
+    slots = (steps + 1) * PIECES
     any_spec = pl.BlockSpec(memory_space=pl.ANY)
     dma = pltpu.SemaphoreType.DMA
     low, wide = jnp.bfloat16, jnp.float32

time: 30.1 us -> 29.7 us (0.987)
  Pallas kernels: 28.9 us -> 28.5 us
    pallas_call x1, Pallas kernels: 28.9 us -> 28.5 us  [fused(): pl.pallas_call(functools.partial(fused_kernel, dp, depth), out_shape=pltp...]
where the time goes in v6:
time: 29.7 us; the launch traced here: 29.5 us
  Pallas kernels  28.5 us (96%)
  local copies, waits for them, and re-layouts  0.98 us (3%)
    pallas_call x1, Pallas kernels, fused(): pl.pallas_call(functools.partial(fused_kernel, dp, depth), out_shape=pltp...  28.5 us
    unnamed x1, local copies, waits for them, and re-layouts  0.98 us

profile of v6, /device:TPU:0, one launch (start us, length us, event | category | flops | bytes accessed | tf_op | source)
XLA Modules:
  0.0 29.5 jit_solution(704368780114536848)
XLA Ops:
  0.0 28.5 %shard_map.55 = bf16[2112,256]{1,0:T(8,128)(2,1)S(1)} custom-call(bf16[256,1024]{1,0:T(8,128)(2,1)} %bitcast.10, bf16[256,1024]{1,0:T(8,128)(2,1)} %bitcast.11, bf16[256,1024]{1,0:T(8,128)(2,1)} %bitcast.12, f32[4,1024]{1,0:T(4,128)} %bitcast.13, bf16[264,1024]{1,0:T(8,128)(2,1)} %bitcast.9), custom_call_target="tpu_custom_call" | custom-call | tf_op jit(solution)/shard_map/pallas_call | solution.py:391
  28.5 1.0 %copy.7 = bf16[1,256,2112]{1,2,0:T(8,128)(2,1)} copy(bf16[1,256,2112]{1,2,0:T(8,128)(2,1)S(1)} %bitcast.8) | data formatting | bytes 2162688
